TPU v7x, 32 devices: a whole 2x2x4 slice. The times are simulated.
32 devices in a mesh: ep: 8 (over z, core), tp: 4 (over y, x).
Axes of the slice: x: 2, y: 2, z: 4, core: 2. Of those that a mesh axis runs over, the one named last changes fastest.
Arguments:
- tokens: bfloat16 [2048, 2048], P('ep'), may hold values from -6 to 6
- norm_gain: float32 [2048], replicated, may hold values from 0.1 to 1.9
- route_ids: int32 [2048, 4], P('ep'), may hold values from 0 to 15, all different within a row; in each aligned block of 256 rows (0 to 255, 256 to 511, ...) at most 96 rows name the same one
- route_weights: float32 [2048, 4], P('ep'), may hold values from 0.1 to 1
- w_gate: bfloat16 [16, 2048, 2048], P('ep', None, 'tp'), may hold values from -0.33007812 to 0.33007812
- w_up: bfloat16 [16, 2048, 2048], P('ep', None, 'tp'), may hold values from -0.33007812 to 0.33007812
- w_down: bfloat16 [16, 2048, 2048], P('ep', None, 'tp'), may hold values from -0.026489258 to 0.026489258
Outputs:
- mixed_out: bfloat16 [2048, 2048], P('ep', 'tp')
Inputs may be any that keep to these rules, and one draw needn't show every extreme that they name: `route_ids`: each token names 4 different experts. Within the tokens of one index of ep (aligned blocks of 256 tokens) no expert is named more than 96 times, a bound that some block reaches.
All inputs are finite; a program needn't handle non-finite values.
Results may differ from a plain program's by a relative error of at most 0.007.
Values may be sent and summed in bfloat16 or wider, within the bound.
A program may use at most 64 MiB of HBM per device.

v0:
```python
import jax
import jax.numpy as jnp
from jax import lax
from jax.sharding import PartitionSpec as P

swiglu_limit = 7.0
swiglu_alpha = 1.702
norm_eps = 1e-05


def clamped_units(gate_pre, up_pre):
    capped = jnp.minimum(gate_pre, swiglu_limit)
    linear = jnp.clip(up_pre, -swiglu_limit, swiglu_limit)
    return capped * jax.nn.sigmoid(swiglu_alpha * capped) * (linear + 1.0)


def expert_work(outgoing, gate_weight, up_weight, down_weight):
    received = lax.all_to_all(outgoing, "ep", split_axis=1, concat_axis=1, tiled=True)
    local_count, sources, capacity, columns = received.shape
    row_count = sources * capacity
    row_block = received.reshape(local_count, row_count, columns)
    shard_piece = lax.all_gather(row_block, "tp", axis=2, tiled=True)
    gate_sum = jnp.einsum(
        "lrd,ldf->lrf", shard_piece, gate_weight, preferred_element_type=jnp.float32
    )
    up_sum = jnp.einsum("lrd,ldf->lrf", shard_piece, up_weight, preferred_element_type=jnp.float32)
    activation = clamped_units(gate_sum, up_sum).astype(jnp.bfloat16)
    out_cols = down_weight.shape[2]
    result = jnp.einsum(
        "lrf,lfd->lrd",
        lax.all_gather(activation, "tp", axis=2, tiled=True),
        down_weight,
        preferred_element_type=jnp.float32,
    )
    result = result.astype(jnp.bfloat16).reshape(local_count, sources, capacity, out_cols)
    return lax.all_to_all(result, "ep", split_axis=1, concat_axis=1, tiled=True)


def per_device(tokens, norm_gain, route_ids, route_weights, w_gate, w_up, w_down):
    local_count = w_gate.shape[0]
    sources = lax.axis_size("ep")
    tp_count = lax.axis_size("tp")
    width = tokens.shape[1]
    columns = width // tp_count
    experts = local_count * sources
    tok_rows, top_count = route_ids.shape
    capacity = 3 * tok_rows * top_count // (2 * experts)
    values = tokens.astype(jnp.float32)
    row_mean = jnp.mean(values, axis=1, keepdims=True)
    centred = values - row_mean
    row_var = jnp.mean(centred * centred, axis=1, keepdims=True)
    offset = lax.axis_index("tp") * columns
    own_cols = lax.dynamic_slice_in_dim(centred, offset, columns, 1)
    own_gain = lax.dynamic_slice_in_dim(norm_gain, offset, columns, 0)
    normed = (own_cols * lax.rsqrt(row_var + norm_eps) * own_gain).astype(jnp.bfloat16)
    flat_ids = route_ids.reshape(-1)
    matches = (flat_ids[:, None] == jnp.arange(experts, dtype=jnp.int32)[None, :]).astype(jnp.int32)
    earlier = jnp.cumsum(matches, axis=0) - matches
    slot_index = jnp.sum(earlier * matches, axis=1)
    position = (
        flat_ids % local_count * (sources * capacity)
        + flat_ids // local_count * capacity
        + slot_index
    )
    buffer_rows = local_count * sources * capacity
    placed = (
        position.reshape(tok_rows, top_count)[:, :, None]
        == jnp.arange(buffer_rows, dtype=jnp.int32)[None, None, :]
    )
    placement_matrix = jnp.any(placed, axis=1).astype(jnp.bfloat16)
    outgoing = jnp.einsum("tp,td->pd", placement_matrix, normed, preferred_element_type=jnp.float32)
    outgoing = outgoing.astype(jnp.bfloat16).reshape(local_count, sources, capacity, columns)
    returned = jnp.concatenate(
        [
            expert_work(
                outgoing[number : number + 1],
                w_gate[number : number + 1],
                w_up[number : number + 1],
                w_down[number : number + 1],
            )
            for number in range(local_count)
        ],
        axis=0,
    )
    flat_out = returned.reshape(buffer_rows, columns)
    picked = flat_out[position].reshape(tok_rows, top_count, columns).astype(jnp.float32)
    return jnp.sum(picked * route_weights[:, :, None], axis=1).astype(jnp.bfloat16)


def solution(mesh):
    return jax.shard_map(
        per_device,
        mesh=mesh,
        in_specs=(
            P("ep", None),
            P(),
            P("ep", None),
            P("ep", None),
            P("ep", None, "tp"),
            P("ep", None, "tp"),
            P("ep", None, "tp"),
        ),
        out_specs=P("ep", "tp"),
        check_vma=False,
    )
```

profile of v0, /device:TPU:0, one launch (start us, length us, event | category | flops | bytes accessed | tf_op | source)
XLA Modules:
  0.0 269.5 jit_solution(14024327743090888040)
XLA Ops:
  6.5 0.9 copy.62
  7.7 4.5 %reduce-window.6 = s32[16,8,128]{2,1,0:T(8,128)S(1)} reduce-window(s32[16,8,128]{2,1,0:T(8,128)S(1)} %fusion.42, s32[]{:T(128)} %constant.28.clone.1), window={size=1x1x128 pad=0_0x0_0x127_0}, to_apply=%region_0.0 | reduce-window | flops 2080768 | bytes 131076 | tf_op jit(solution)/shard_map/reduce-window
  12.3 0.1 copy.64
  12.7 0.1 reduce_sum.41
  12.9 0.7 fusion.45
  13.6 1.7 fusion
  15.3 0.2 convert_reduce_fusion
  15.6 0.4 multiply_reduce_fusion.1
  16.0 0.8 dynamic_slice.7
  16.8 1.7 convolution_convert_fusion
  18.6 27.2 %all_to_all.20 = bf16[1,8,96,512]{3,2,0,1:T(8,128)(2,1)} all-to-all(bf16[1,8,96,512]{3,2,0,1:T(8,128)(2,1)S(1)} %bitcast.82), channel_id=1, replica_groups=mesh['ep'=8,'tp'=4] {'ep'}, dimensions={1} | all-to-all | bytes 1572864 | tf_op jit(solution)/shard_map/all_to_all | solution.py:18
  45.9 24.0 %all_to_all.21 = bf16[1,8,96,512]{3,2,0,1:T(8,128)(2,1)} all-to-all(bf16[1,8,96,512]{3,2,0,1:T(8,128)(2,1)S(1)} %bitcast.81), channel_id=1, replica_groups=mesh['ep'=8,'tp'=4] {'ep'}, dimensions={1} | all-to-all | bytes 1572864 | tf_op jit(solution)/shard_map/all_to_all | solution.py:18
  70.0 18.6 %all-gather.7.cloned.1.call-done = bf16[1,768,2048]{2,1,0:T(8,128)(2,1)} async-done(((bf16[1,768,512]{2,1,0:T(8,128)(2,1)}), bf16[1,768,2048]{2,1,0:T(8,128)(2,1)}) %all-gather.7.cloned.1.call-update) | async-done | bytes 3145744 | tf_op jit(solution)/shard_map/all_gather | solution.py:22
  88.6 4.5 %fusion.7 = f32[768,512]{1,0:T(8,128)S(1)} fusion(bf16[1,768,2048]{2,1,0:T(8,128)(2,1)} %all-gather.7.cloned.1.call-done, bf16[2,2048,512]{2,1,0:T(8,128)(2,1)} %param.11), kind=kOutput, calls=%fused_computation.9 | convolution fusion | flops 1610612736 | bytes 6815744 | tf_op jit(solution)/shard_map/lrd,ldf->lrf/dot_general | solution.py:23
  93.1 0.2 copy-done.5
  93.3 3.0 %multiply_convert_fusion.1 = bf16[768,512]{1,0:T(8,128)(2,1)} fusion(f32[768,512]{1,0:T(8,128)S(1)} %fusion.7, bf16[2,2048,512]{2,1,0:T(8,128)(2,1)S(1)} %copy-done.2, bf16[1,768,2048]{2,1,0:T(8,128)(2,1)S(1)} %copy-done.5), kind=kOutput, calls=%fused_computation.32 | convolution fusion | flops 1614544896 | bytes 7602176 | tf_op jit(solution)/shard_map/lrd,ldf->lrf/dot_general | solution.py:26
  96.4 37.8 %all-gather.9.cloned.1.call-done = bf16[1,768,2048]{2,1,0:T(8,128)(2,1)} async-done(((bf16[1,768,512]{2,1,0:T(8,128)(2,1)}), bf16[1,768,2048]{2,1,0:T(8,128)(2,1)}) %all-gather.9.cloned.1.call-update) | async-done | bytes 3145744 | tf_op jit(solution)/shard_map/all_gather | solution.py:22
  134.2 4.5 %fusion.3 = f32[768,512]{1,0:T(8,128)S(1)} fusion(bf16[1,768,2048]{2,1,0:T(8,128)(2,1)} %all-gather.9.cloned.1.call-done, bf16[2,2048,512]{2,1,0:T(8,128)(2,1)} %param.11), kind=kOutput, calls=%fused_computation.5 | convolution fusion | flops 1610612736 | bytes 6815744 | tf_op jit(solution)/shard_map/lrd,ldf->lrf/dot_general | solution.py:23
  138.7 0.2 copy-done.4
  138.9 3.0 %multiply_convert_fusion = bf16[768,512]{1,0:T(8,128)(2,1)} fusion(f32[768,512]{1,0:T(8,128)S(1)} %fusion.3, bf16[2,2048,512]{2,1,0:T(8,128)(2,1)S(1)} %copy-done.3, bf16[1,768,2048]{2,1,0:T(8,128)(2,1)S(1)} %copy-done.4), kind=kOutput, calls=%fused_computation.31 | convolution fusion | flops 1614544896 | bytes 7602176 | tf_op jit(solution)/shard_map/lrd,ldf->lrf/dot_general | solution.py:26
  141.9 37.8 %all-gather.11.cloned.1.call-done = bf16[768,2048]{1,0:T(8,128)(2,1)} async-done(((bf16[768,512]{1,0:T(8,128)(2,1)}), bf16[768,2048]{1,0:T(8,128)(2,1)}) %all-gather.11.cloned.1.call-update) | async-done | bytes 3145744 | tf_op jit(solution)/shard_map/all_gather | solution.py:31
  179.8 5.2 %fusion.31 = bf16[768,512]{1,0:T(8,128)(2,1)} fusion(bf16[768,2048]{1,0:T(8,128)(2,1)} %all-gather.11.cloned.1.call-done, bf16[2,2048,512]{2,1,0:T(8,128)(2,1)} %param.13), kind=kOutput, calls=%fused_computation.33 | convolution fusion | flops 1611005952 | bytes 6029312 | tf_op jit(solution)/shard_map/lrf,lfd->lrd/dot_general | solution.py:29
  185.0 4.6 %all-to-all-start.1 = ((bf16[1,8,96,512]{3,2,0,1:T(8,128)(2,1)}), bf16[1,8,96,512]{3,2,0,1:T(8,128)(2,1)S(1)}, u32[]{:S(2)}, u32[]{:S(2)}) async-start(bf16[1,8,96,512]{3,2,0,1:T(8,128)(2,1)} %bitcast.10), calls=%async_computation.1 | async-start | bytes 1572864 | tf_op jit(solution)/shard_map/all_to_all | solution.py:36
  189.6 35.6 %all-gather.13.cloned.1.call-done = bf16[768,2048]{1,0:T(8,128)(2,1)} async-done(((bf16[768,512]{1,0:T(8,128)(2,1)}), bf16[768,2048]{1,0:T(8,128)(2,1)}) %all-gather.13.cloned.1.call-update) | async-done | bytes 3145744 | tf_op jit(solution)/shard_map/all_gather | solution.py:31
  225.2 5.2 %fusion.34 = bf16[768,512]{1,0:T(8,128)(2,1)} fusion(bf16[768,2048]{1,0:T(8,128)(2,1)} %all-gather.13.cloned.1.call-done, bf16[2,2048,512]{2,1,0:T(8,128)(2,1)} %param.13), kind=kOutput, calls=%fused_computation.34 | convolution fusion | flops 1611005952 | bytes 6029312 | tf_op jit(solution)/shard_map/lrf,lfd->lrd/dot_general | solution.py:29
  230.4 4.6 %all-to-all-start.3 = ((bf16[1,8,96,512]{3,2,0,1:T(8,128)(2,1)}), bf16[1,8,96,512]{3,2,0,1:T(8,128)(2,1)S(1)}, u32[]{:S(2)}, u32[]{:S(2)}) async-start(bf16[1,8,96,512]{3,2,0,1:T(8,128)(2,1)} %bitcast.19), calls=%async_computation.3 | async-start | bytes 1572864 | tf_op jit(solution)/shard_map/all_to_all | solution.py:36
  235.1 0.1 copy.73
  235.3 20.6 %all-to-all-done.3 = bf16[1,8,96,512]{3,2,0,1:T(8,128)(2,1)S(1)} async-done(((bf16[1,8,96,512]{3,2,0,1:T(8,128)(2,1)}), bf16[1,8,96,512]{3,2,0,1:T(8,128)(2,1)S(1)}, u32[]{:S(2)}, u32[]{:S(2)}) %all-to-all-start.3) | async-done | bytes 786464 | tf_op jit(solution)/shard_map/all_to_all | solution.py:36
  255.9 0.1 pad_maximum_fusion
  256.2 4.0 %gather_fusion = bf16[1024,512]{1,0:T(8,128)(2,1)S(1)} fusion(bf16[1536,512]{1,0:T(8,128)(2,1)S(1)} %bitcast.78, s32[1024]{0:T(1024)S(1)} %broadcast_clamp_fusion), kind=kCustom, calls=%fused_computation | custom fusion | bytes 2101248 | tf_op jit(solution)/shard_map/gather | solution.py:86
  260.2 0.7 reshape.290
  260.9 2.1 multiply_reduce_fusion
  (36 shorter events, 1.2 us)
Async XLA Ops:
  6.5 8.8 %copy-start = (bf16[256,2048]{1,0:T(8,128)(2,1)S(1)}, bf16[256,2048]{1,0:T(8,128)(2,1)}, u32[]{:S(2)}) copy-start(bf16[256,2048]{1,0:T(8,128)(2,1)} %param.7) | copy-start | bytes 3145732
  6.5 82.1 %all-gather.7.cloned.1.call-start = ((), (), s32[]{:S(2)}) async-start(), calls=%async_computation.4 | async-start | bytes 3932160 | tf_op jit(solution)/shard_map/all_gather | solution.py:22
  45.8 88.4 %all-gather.9.cloned.1.call-start = ((), (), s32[]{:S(2)}) async-start(), calls=%async_computation.5 | async-start | bytes 3932160 | tf_op jit(solution)/shard_map/all_gather | solution.py:22
  69.9 109.8 %all-gather.11.cloned.1.call-start = ((), (), s32[]{:S(2)}) async-start(), calls=%async_computation.6 | async-start | bytes 3932160 | tf_op jit(solution)/shard_map/all_gather | solution.py:31
  88.6 4.5 %copy-start.2 = (bf16[2,2048,512]{2,1,0:T(8,128)(2,1)S(1)}, bf16[2,2048,512]{2,1,0:T(8,128)(2,1)}, u32[]{:S(2)}) copy-start(bf16[2,2048,512]{2,1,0:T(8,128)(2,1)} %param.12) | copy-start | bytes 12582916
  88.6 4.7 %copy-start.5 = (bf16[1,768,2048]{2,1,0:T(8,128)(2,1)S(1)}, bf16[1,768,2048]{2,1,0:T(8,128)(2,1)}, u32[]{:S(2)}) copy-start(bf16[1,768,2048]{2,1,0:T(8,128)(2,1)} %all-gather.7.cloned.1.call-done) | copy-start | bytes 9437188
  96.4 128.8 %all-gather.13.cloned.1.call-start = ((), (), s32[]{:S(2)}) async-start(), calls=%async_computation.7 | async-start | bytes 3932160 | tf_op jit(solution)/shard_map/all_gather | solution.py:31
  134.2 4.5 %copy-start.3 = (bf16[2,2048,512]{2,1,0:T(8,128)(2,1)S(1)}, bf16[2,2048,512]{2,1,0:T(8,128)(2,1)}, u32[]{:S(2)}) copy-start(bf16[2,2048,512]{2,1,0:T(8,128)(2,1)} %param.12) | copy-start | bytes 12582916
  134.2 4.7 %copy-start.4 = (bf16[1,768,2048]{2,1,0:T(8,128)(2,1)S(1)}, bf16[1,768,2048]{2,1,0:T(8,128)(2,1)}, u32[]{:S(2)}) copy-start(bf16[1,768,2048]{2,1,0:T(8,128)(2,1)} %all-gather.9.cloned.1.call-done) | copy-start | bytes 9437188
  185.0 45.4 %all-to-all-start.1 = ((bf16[1,8,96,512]{3,2,0,1:T(8,128)(2,1)}), bf16[1,8,96,512]{3,2,0,1:T(8,128)(2,1)S(1)}, u32[]{:S(2)}, u32[]{:S(2)}) async-start(bf16[1,8,96,512]{3,2,0,1:T(8,128)(2,1)} %bitcast.10), calls=%async_computation.1 | async-start | bytes 1572864 | tf_op jit(solution)/shard_map/all_to_all | solution.py:36
  189.6 45.5 %copy-start.1 = (f32[256,4]{0,1:T(4,128)S(1)}, f32[256,4]{0,1:T(4,128)}, u32[]{:S(2)}) copy-start(f32[256,4]{0,1:T(4,128)} %param.10) | copy-start | bytes 12292
  230.4 25.6 %all-to-all-start.3 = ((bf16[1,8,96,512]{3,2,0,1:T(8,128)(2,1)}), bf16[1,8,96,512]{3,2,0,1:T(8,128)(2,1)S(1)}, u32[]{:S(2)}, u32[]{:S(2)}) async-start(bf16[1,8,96,512]{3,2,0,1:T(8,128)(2,1)} %bitcast.19), calls=%async_computation.3 | async-start | bytes 1572864 | tf_op jit(solution)/shard_map/all_to_all | solution.py:36
Sparse Core Ops, SparseCore 0:
  45.9 42.6 all-gather.6
  90.4 43.6 all-gather.8
  136.0 43.6 all-gather.10
  181.4 43.6 all-gather.12
where the time goes:
time: 270 us; the launch traced here: 269 us
  waiting for transfers between devices  150 us (56%)
  blocking collectives  51.2 us (19%)
  matrix products  27 us (10%)
  between operations  13.3 us (5%)
  other arithmetic  10 us (4%)
  starting transfers between devices  9.36 us (3%)
  local copies, waits for them, and re-layouts  8.03 us (3%)
    all_gather x2, waiting for transfers between devices, expert_work(): lax.all_gather(activation, 'tp', axis=2, tiled=True)  73.4 us
    all_gather x2, waiting for transfers between devices, expert_work(): shard_piece = lax.all_gather(row_block, 'tp', axis=2, tiled=True)  56.4 us
    all_to_all x2, blocking collectives, expert_work(): lax.all_to_all(outgoing, 'ep', split_axis=1, concat_axis=1, tiled=True)  51.2 us
    all_to_all x2, waiting for transfers between devices, expert_work(): return lax.all_to_all(result, 'ep', split_axis=1, concat_axis=1, tiled=True)  20.6 us
    dot_general x2, matrix products, expert_work(): jnp.einsum('lrf,lfd->lrd', lax.all_gather(activation, 'tp', axis=2, tiled...  10.4 us
    all_to_all x2, starting transfers between devices, expert_work(): return lax.all_to_all(result, 'ep', split_axis=1, concat_axis=1, tiled=True)  9.23 us
    dot_general x2, matrix products, expert_work(): jnp.einsum('lrd,ldf->lrf', shard_piece, gate_weight, preferred_element_ty...  8.95 us
    dot_general x2, matrix products, expert_work(): jnp.einsum('lrd,ldf->lrf', shard_piece, up_weight, preferred_element_type...  5.99 us
  transfers between devices with their start and end apart: 6, of which 5 were waited for; matrix products, arithmetic and copies ran while one was open for 10% of the time, Pallas kernels for 0%

commit v1 on v0

--- a/solution.py
+++ b/solution.py
@@ -33,7 +33,10 @@
         preferred_element_type=jnp.float32,
     )
     result = result.astype(jnp.bfloat16).reshape(local_count, sources, capacity, out_cols)
-    return lax.all_to_all(result, "ep", split_axis=1, concat_axis=1, tiled=True)
+    return jnp.concatenate(
+        lax.all_to_all(jnp.stack(jnp.split(result, lax.axis_size("ep"), axis=1)), "ep", 0, 0),
+        axis=1,
+    )
 
 
 def per_device(tokens, norm_gain, route_ids, route_weights, w_gate, w_up, w_down):

time: 270 us -> 274 us (1.015)
  local copies, waits for them, and re-layouts: 8.03 us -> 18.2 us
  waiting for transfers between devices: 150 us -> 146 us
    unnamed x14 -> x28, local copies, waits for them, and re-layouts: 1.54 us -> 10.5 us
    all_gather x2, waiting for transfers between devices: 73.4 us -> 69.2 us  [expert_work(): lax.all_gather(activation, 'tp', axis=2, tiled=True)]
  transfers between devices with their start and end apart: 6 -> 6, of which waited for: 5 -> 5; matrix products, arithmetic and copies ran while one was open for 10% -> 12% of each run, Pallas kernels for 0% -> 0%
where the time goes in v1:
time: 274 us
  waiting for transfers between devices  146 us (53%)
  blocking collectives  51.2 us (19%)
  matrix products  25.3 us (9%)
  local copies, waits for them, and re-layouts  18.2 us (7%)
  between operations  13.3 us (5%)
  other arithmetic  10 us (4%)
  starting transfers between devices  9.37 us (3%)
    all_gather x2, waiting for transfers between devices, expert_work(): lax.all_gather(activation, 'tp', axis=2, tiled=True)  69.2 us
    all_gather x2, waiting for transfers between devices, expert_work(): shard_piece = lax.all_gather(row_block, 'tp', axis=2, tiled=True)  56.4 us
    all_to_all x2, blocking collectives, expert_work(): lax.all_to_all(outgoing, 'ep', split_axis=1, concat_axis=1, tiled=True)  51.2 us
    all_to_all x2, waiting for transfers between devices, expert_work(): lax.all_to_all(jnp.stack(jnp.split(result, lax.axis_size('ep'), axis=1)),...  20.6 us
    unnamed x28, local copies, waits for them, and re-layouts  10.5 us
    all_to_all x2, starting transfers between devices, expert_work(): lax.all_to_all(jnp.stack(jnp.split(result, lax.axis_size('ep'), axis=1)),...  9.24 us
    dot_general x2, matrix products, expert_work(): jnp.einsum('lrd,ldf->lrf', shard_piece, gate_weight, preferred_element_ty...  8.95 us
    dot_general x2, matrix products, expert_work(): jnp.einsum('lrf,lfd->lrd', lax.all_gather(activation, 'tp', axis=2, tiled...  8.64 us
  transfers between devices with their start and end apart: 6, of which 5 were waited for; matrix products, arithmetic and copies ran while one was open for 12% of the time, Pallas kernels for 0%

profile of v1, /device:TPU:0, one launch (start us, length us, event | category | flops | bytes accessed | tf_op | source)
XLA Modules:
  0.0 273.6 jit_solution(14410275814470723757)
XLA Ops:
  6.5 0.9 copy.92
  7.7 4.5 %reduce-window.6 = s32[16,8,128]{2,1,0:T(8,128)S(1)} reduce-window(s32[16,8,128]{2,1,0:T(8,128)S(1)} %fusion.58, s32[]{:T(128)} %constant.28.clone.1), window={size=1x1x128 pad=0_0x0_0x127_0}, to_apply=%region_0.0 | reduce-window | flops 2080768 | bytes 131076 | tf_op jit(solution)/shard_map/reduce-window
  12.9 0.7 fusion.61
  13.6 1.7 fusion
  16.0 0.8 dynamic_slice.7
  16.8 1.7 convolution_convert_fusion
  18.6 27.2 %all_to_all.20 = bf16[1,8,96,512]{3,2,0,1:T(8,128)(2,1)} all-to-all(bf16[1,8,96,512]{3,2,0,1:T(8,128)(2,1)S(1)} %bitcast.146), channel_id=1, replica_groups=mesh['ep'=8,'tp'=4] {'ep'}, dimensions={1} | all-to-all | bytes 1572864 | tf_op jit(solution)/shard_map/all_to_all | solution.py:18
  45.9 24.0 %all_to_all.21 = bf16[1,8,96,512]{3,2,0,1:T(8,128)(2,1)} all-to-all(bf16[1,8,96,512]{3,2,0,1:T(8,128)(2,1)S(1)} %bitcast.145), channel_id=1, replica_groups=mesh['ep'=8,'tp'=4] {'ep'}, dimensions={1} | all-to-all | bytes 1572864 | tf_op jit(solution)/shard_map/all_to_all | solution.py:18
  70.0 18.6 %all-gather.7.cloned.1.call-done = bf16[1,768,2048]{2,1,0:T(8,128)(2,1)} async-done(((bf16[1,768,512]{2,1,0:T(8,128)(2,1)}), bf16[1,768,2048]{2,1,0:T(8,128)(2,1)}) %all-gather.7.cloned.1.call-update) | async-done | bytes 3145744 | tf_op jit(solution)/shard_map/all_gather | solution.py:22
  88.6 4.5 %fusion.7 = f32[768,512]{1,0:T(8,128)S(1)} fusion(bf16[1,768,2048]{2,1,0:T(8,128)(2,1)} %all-gather.7.cloned.1.call-done, bf16[2,2048,512]{2,1,0:T(8,128)(2,1)} %param.11), kind=kOutput, calls=%fused_computation.9 | convolution fusion | flops 1610612736 | bytes 6815744 | tf_op jit(solution)/shard_map/lrd,ldf->lrf/dot_general | solution.py:23
  93.3 3.0 %multiply_convert_fusion.1 = bf16[768,512]{1,0:T(8,128)(2,1)} fusion(f32[768,512]{1,0:T(8,128)S(1)} %fusion.7, bf16[2,2048,512]{2,1,0:T(8,128)(2,1)S(1)} %copy-done.2, bf16[1,768,2048]{2,1,0:T(8,128)(2,1)S(1)} %copy-done.5), kind=kOutput, calls=%fused_computation.32 | convolution fusion | flops 1614544896 | bytes 7602176 | tf_op jit(solution)/shard_map/lrd,ldf->lrf/dot_general | solution.py:26
  96.4 37.8 %all-gather.9.cloned.1.call-done = bf16[1,768,2048]{2,1,0:T(8,128)(2,1)} async-done(((bf16[1,768,512]{2,1,0:T(8,128)(2,1)}), bf16[1,768,2048]{2,1,0:T(8,128)(2,1)}) %all-gather.9.cloned.1.call-update) | async-done | bytes 3145744 | tf_op jit(solution)/shard_map/all_gather | solution.py:22
  134.2 4.5 %fusion.3 = f32[768,512]{1,0:T(8,128)S(1)} fusion(bf16[1,768,2048]{2,1,0:T(8,128)(2,1)} %all-gather.9.cloned.1.call-done, bf16[2,2048,512]{2,1,0:T(8,128)(2,1)} %param.11), kind=kOutput, calls=%fused_computation.5 | convolution fusion | flops 1610612736 | bytes 6815744 | tf_op jit(solution)/shard_map/lrd,ldf->lrf/dot_general | solution.py:23
  138.9 3.0 %multiply_convert_fusion = bf16[768,512]{1,0:T(8,128)(2,1)} fusion(f32[768,512]{1,0:T(8,128)S(1)} %fusion.3, bf16[2,2048,512]{2,1,0:T(8,128)(2,1)S(1)} %copy-done.3, bf16[1,768,2048]{2,1,0:T(8,128)(2,1)S(1)} %copy-done.4), kind=kOutput, calls=%fused_computation.31 | convolution fusion | flops 1614544896 | bytes 7602176 | tf_op jit(solution)/shard_map/lrd,ldf->lrf/dot_general | solution.py:26
  141.9 37.8 %all-gather.11.cloned.1.call-done = bf16[768,2048]{1,0:T(8,128)(2,1)} async-done(((bf16[768,512]{1,0:T(8,128)(2,1)}), bf16[768,2048]{1,0:T(8,128)(2,1)}) %all-gather.11.cloned.1.call-update) | async-done | bytes 3145744 | tf_op jit(solution)/shard_map/all_gather | solution.py:31
  179.8 4.3 %fusion.31 = bf16[768,512]{1,0:T(8,128)(2,1)S(1)} fusion(bf16[768,2048]{1,0:T(8,128)(2,1)} %all-gather.11.cloned.1.call-done, bf16[2,2048,512]{2,1,0:T(8,128)(2,1)} %param.13), kind=kOutput, calls=%fused_computation.33 | convolution fusion | flops 1611005952 | bytes 6029312 | tf_op jit(solution)/shard_map/lrf,lfd->lrd/dot_general | solution.py:29
  184.1 0.6 fusion.54
  185.4 0.6 fusion.52
  186.0 0.6 fusion.51
  187.9 0.6 fusion.48
  189.2 4.6 %all-to-all-start.1 = ((bf16[8,1,1,96,512]{4,3,2,1,0:T(8,128)(2,1)}), bf16[8,1,1,96,512]{4,3,2,1,0:T(8,128)(2,1)S(1)}, u32[]{:S(2)}, u32[]{:S(2)}) async-start(bf16[8,1,1,96,512]{4,3,2,1,0:T(8,128)(2,1)} %fusion.47), calls=%async_computation.1 | async-start | bytes 1572864 | tf_op jit(solution)/shard_map/all_to_all | solution.py:37
  193.8 31.4 %all-gather.13.cloned.1.call-done = bf16[768,2048]{1,0:T(8,128)(2,1)} async-done(((bf16[768,512]{1,0:T(8,128)(2,1)}), bf16[768,2048]{1,0:T(8,128)(2,1)}) %all-gather.13.cloned.1.call-update) | async-done | bytes 3145744 | tf_op jit(solution)/shard_map/all_gather | solution.py:31
  225.2 4.3 %fusion.34 = bf16[768,512]{1,0:T(8,128)(2,1)S(1)} fusion(bf16[768,2048]{1,0:T(8,128)(2,1)} %all-gather.13.cloned.1.call-done, bf16[2,2048,512]{2,1,0:T(8,128)(2,1)} %param.13), kind=kOutput, calls=%fused_computation.34 | convolution fusion | flops 1611005952 | bytes 6029312 | tf_op jit(solution)/shard_map/lrf,lfd->lrd/dot_general | solution.py:29
  230.1 0.6 fusion.45
  230.8 0.6 fusion.44
  231.4 0.6 fusion.43
  233.4 0.6 fusion.40
  234.7 4.6 %all-to-all-start.3 = ((bf16[8,1,1,96,512]{4,3,2,1,0:T(8,128)(2,1)}), bf16[8,1,1,96,512]{4,3,2,1,0:T(8,128)(2,1)S(1)}, u32[]{:S(2)}, u32[]{:S(2)}) async-start(bf16[8,1,1,96,512]{4,3,2,1,0:T(8,128)(2,1)} %fusion.39), calls=%async_computation.3 | async-start | bytes 1572864 | tf_op jit(solution)/shard_map/all_to_all | solution.py:37
  239.6 20.6 %all-to-all-done.3 = bf16[8,1,1,96,512]{4,3,2,1,0:T(8,128)(2,1)S(1)} async-done(((bf16[8,1,1,96,512]{4,3,2,1,0:T(8,128)(2,1)}), bf16[8,1,1,96,512]{4,3,2,1,0:T(8,128)(2,1)S(1)}, u32[]{:S(2)}, u32[]{:S(2)}) %all-to-all-start.3) | async-done | bytes 786464 | tf_op jit(solution)/shard_map/all_to_all | solution.py:37
  260.4 4.0 %gather_fusion = bf16[1024,512]{1,0:T(8,128)(2,1)S(1)} fusion(bf16[1536,512]{1,0:T(8,128)(2,1)S(1)} %bitcast.140, s32[1024]{0:T(1024)S(1)} %broadcast_clamp_fusion), kind=kCustom, calls=%fused_computation | custom fusion | bytes 2101248 | tf_op jit(solution)/shard_map/gather | solution.py:89
  264.3 0.7 reshape.298
  265.0 2.1 multiply_reduce_fusion
  (51 shorter events, 7.9 us)
Async XLA Ops:
  6.5 8.8 %copy-start = (bf16[256,2048]{1,0:T(8,128)(2,1)S(1)}, bf16[256,2048]{1,0:T(8,128)(2,1)}, u32[]{:S(2)}) copy-start(bf16[256,2048]{1,0:T(8,128)(2,1)} %param.7) | copy-start | bytes 3145732
  6.5 82.1 %all-gather.7.cloned.1.call-start = ((), (), s32[]{:S(2)}) async-start(), calls=%async_computation.4 | async-start | bytes 3932160 | tf_op jit(solution)/shard_map/all_gather | solution.py:22
  45.8 88.4 %all-gather.9.cloned.1.call-start = ((), (), s32[]{:S(2)}) async-start(), calls=%async_computation.5 | async-start | bytes 3932160 | tf_op jit(solution)/shard_map/all_gather | solution.py:22
  69.9 109.8 %all-gather.11.cloned.1.call-start = ((), (), s32[]{:S(2)}) async-start(), calls=%async_computation.6 | async-start | bytes 3932160 | tf_op jit(solution)/shard_map/all_gather | solution.py:31
  88.6 4.5 %copy-start.2 = (bf16[2,2048,512]{2,1,0:T(8,128)(2,1)S(1)}, bf16[2,2048,512]{2,1,0:T(8,128)(2,1)}, u32[]{:S(2)}) copy-start(bf16[2,2048,512]{2,1,0:T(8,128)(2,1)} %param.12) | copy-start | bytes 12582916
  88.6 4.7 %copy-start.5 = (bf16[1,768,2048]{2,1,0:T(8,128)(2,1)S(1)}, bf16[1,768,2048]{2,1,0:T(8,128)(2,1)}, u32[]{:S(2)}) copy-start(bf16[1,768,2048]{2,1,0:T(8,128)(2,1)} %all-gather.7.cloned.1.call-done) | copy-start | bytes 9437188
  96.4 128.8 %all-gather.13.cloned.1.call-start = ((), (), s32[]{:S(2)}) async-start(), calls=%async_computation.7 | async-start | bytes 3932160 | tf_op jit(solution)/shard_map/all_gather | solution.py:31
  134.2 4.5 %copy-start.3 = (bf16[2,2048,512]{2,1,0:T(8,128)(2,1)S(1)}, bf16[2,2048,512]{2,1,0:T(8,128)(2,1)}, u32[]{:S(2)}) copy-start(bf16[2,2048,512]{2,1,0:T(8,128)(2,1)} %param.12) | copy-start | bytes 12582916
  134.2 4.7 %copy-start.4 = (bf16[1,768,2048]{2,1,0:T(8,128)(2,1)S(1)}, bf16[1,768,2048]{2,1,0:T(8,128)(2,1)}, u32[]{:S(2)}) copy-start(bf16[1,768,2048]{2,1,0:T(8,128)(2,1)} %all-gather.9.cloned.1.call-done) | copy-start | bytes 9437188
  189.2 45.5 %all-to-all-start.1 = ((bf16[8,1,1,96,512]{4,3,2,1,0:T(8,128)(2,1)}), bf16[8,1,1,96,512]{4,3,2,1,0:T(8,128)(2,1)S(1)}, u32[]{:S(2)}, u32[]{:S(2)}) async-start(bf16[8,1,1,96,512]{4,3,2,1,0:T(8,128)(2,1)} %fusion.47), calls=%async_computation.1 | async-start | bytes 1572864 | tf_op jit(solution)/shard_map/all_to_all | solution.py:37
  229.5 9.9 %copy-start.1 = (f32[256,4]{0,1:T(4,128)S(1)}, f32[256,4]{0,1:T(4,128)}, u32[]{:S(2)}) copy-start(f32[256,4]{0,1:T(4,128)} %param.10) | copy-start | bytes 12292
  234.7 25.6 %all-to-all-start.3 = ((bf16[8,1,1,96,512]{4,3,2,1,0:T(8,128)(2,1)}), bf16[8,1,1,96,512]{4,3,2,1,0:T(8,128)(2,1)S(1)}, u32[]{:S(2)}, u32[]{:S(2)}) async-start(bf16[8,1,1,96,512]{4,3,2,1,0:T(8,128)(2,1)} %fusion.39), calls=%async_computation.3 | async-start | bytes 1572864 | tf_op jit(solution)/shard_map/all_to_all | solution.py:37
Sparse Core Ops, SparseCore 0:
  45.9 42.6 all-gather.6
  90.4 43.6 all-gather.8
  136.0 43.7 all-gather.10
  181.4 43.6 all-gather.12
